TPU v7x, 32 devices: a whole 2x2x4 slice. The times are simulated.
32 devices in a mesh: ep: 8 (over z, x), tp: 4 (over y, core).
Axes of the slice: x: 2, y: 2, z: 4, core: 2. Of those that a mesh axis runs over, the one named last changes fastest.
Arguments:
- tokens: bfloat16 [192, 4096], P('ep'), may hold values from -6 to 6
- delta_state: float32 [192, 16, 128, 128], P('ep', 'tp'), may hold values from -0.625 to 0.625
- attn_gain: float32 [4096], replicated, may hold values from 0.1 to 1.9
- query_weight: bfloat16 [4096, 2048], P('ep', 'tp'), may hold values from -0.09375 to 0.09375
- key_weight: bfloat16 [4096, 2048], P('ep', 'tp'), may hold values from -0.09375 to 0.09375
- value_weight: bfloat16 [4096, 2048], P('ep', 'tp'), may hold values from -0.09375 to 0.09375
- decay_weight: bfloat16 [4096, 16], replicated, may hold values from -0.09375 to 0.09375
- beta_weight: bfloat16 [4096, 16], replicated, may hold values from -0.09375 to 0.09375
- decay_rate: float32 [16], P('tp'), may hold values from 0.05 to 3
- head_gain: float32 [128], replicated, may hold values from 0.1 to 1.9
- output_weight: bfloat16 [2048, 4096], P('tp'), may hold values from -0.125 to 0.125
- ffn_gain: float32 [4096], replicated, may hold values from 0.1 to 1.9
- expert_ids: int32 [192, 2], P('ep'), may hold values from 0 to 7, all different within a row; in each aligned block of 24 rows (0 to 23, 24 to 47, ...) at most 12 rows name the same one
- group_prob: float32 [192], P('ep'), may hold values from 0.3 to 1
- expert_logit: float32 [192, 2], P('ep'), may hold values from -8 to 8
- expert_gate: bfloat16 [8, 4096, 1024], P('ep', None, 'tp'), may hold values from -0.09375 to 0.09375
- expert_up: bfloat16 [8, 4096, 1024], P('ep', None, 'tp'), may hold values from -0.09375 to 0.09375
- expert_down: bfloat16 [8, 1024, 4096], P('ep', 'tp'), may hold values from -0.1875 to 0.1875
- dense_gate: bfloat16 [4096, 4096], P('tp', 'ep'), may hold values from -0.09375 to 0.09375
- dense_up: bfloat16 [4096, 4096], P('tp', 'ep'), may hold values from -0.09375 to 0.09375
- dense_down: bfloat16 [4096, 4096], P('ep', 'tp'), may hold values from -0.09375 to 0.09375
- dense_mix: float32 [4096], P('tp'), may hold values from -3 to 3
Outputs:
- mixed_out: bfloat16 [192, 4096], P('ep', 'tp')
- new_state: float32 [192, 16, 128, 128], P('ep', 'tp')
Inputs may be any that keep to these rules, and one draw needn't show every extreme that they name: `expert_ids`: each row names 2 different experts. Among the rows of one device (aligned blocks of 24 rows) no expert is named by more than 12 rows, and in every draw some expert reaches 12 in some block.
All inputs are finite; a program needn't handle non-finite values.
Results may differ from a plain program's by a relative error of at most 0.02.
Values may be sent and summed in bfloat16 or wider, within the bound.
A program may use at most 64 MiB of HBM per device.

v0:
```python
import jax
import jax.numpy as jnp
from jax import lax
from jax.sharding import PartitionSpec as P

EPS = 1e-06


def rms_scale(values, gain):
    mean_sq = jnp.mean(values * values, axis=-1, keepdims=True)
    return values * lax.rsqrt(mean_sq + EPS) * gain


def unit_rows(values):
    return values * lax.rsqrt(jnp.sum(values * values, axis=-1, keepdims=True) + EPS)


def per_device(
    tokens,
    delta_state,
    attn_gain,
    query_weight,
    key_weight,
    value_weight,
    decay_weight,
    beta_weight,
    decay_rate,
    head_gain,
    output_weight,
    ffn_gain,
    expert_ids,
    group_prob,
    expert_logit,
    expert_gate,
    expert_up,
    expert_down,
    dense_gate,
    dense_up,
    dense_down,
    dense_mix,
):
    seq_rows = tokens.shape[0]
    head_count = delta_state.shape[1]
    head_size = delta_state.shape[2]
    width_local = head_count * head_size
    tp_index = lax.axis_index("tp")
    residual = tokens.astype(jnp.float32)
    normed = rms_scale(residual, attn_gain).astype(jnp.bfloat16)
    spread = lax.all_to_all(normed, "ep", split_axis=1, concat_axis=0, tiled=True)
    joined = jnp.concatenate((query_weight, key_weight, value_weight), axis=1)
    summed = lax.psum_scatter(
        jnp.dot(spread, joined, preferred_element_type=jnp.float32).astype(jnp.bfloat16),
        "ep",
        scatter_dimension=0,
        tiled=True,
    ).astype(jnp.float32)
    query_sum = summed[:, :width_local]
    key_sum = summed[:, width_local : 2 * width_local]
    value_sum = summed[:, 2 * width_local :]

    def heads_of(values):
        rounded = lax.optimization_barrier(values.astype(jnp.bfloat16))
        return rounded.astype(jnp.float32).reshape(seq_rows, head_count, head_size)

    query_unit = unit_rows(heads_of(query_sum)) * head_size ** (-0.5)
    key_unit = unit_rows(heads_of(key_sum))
    value_heads = heads_of(value_sum)
    decay_cols = lax.dynamic_slice_in_dim(decay_weight, tp_index * head_count, head_count, 1)
    beta_cols = lax.dynamic_slice_in_dim(beta_weight, tp_index * head_count, head_count, 1)
    decay_pre = jnp.dot(normed, decay_cols, preferred_element_type=jnp.float32)
    decay = jnp.exp(-decay_rate * jax.nn.softplus(decay_pre))
    beta_gate = jax.nn.sigmoid(jnp.dot(normed, beta_cols, preferred_element_type=jnp.float32))
    recalled = jnp.einsum("bhk,bhkv->bhv", key_unit, delta_state, precision=lax.Precision.HIGHEST)
    correction = beta_gate[..., None] * (value_heads - decay[..., None] * recalled)
    new_state = (
        decay[..., None, None] * delta_state + key_unit[..., :, None] * correction[..., None, :]
    )
    read_out = jnp.einsum("bhk,bhkv->bhv", query_unit, new_state, precision=lax.Precision.HIGHEST)
    head_out = rms_scale(read_out, head_gain).astype(jnp.bfloat16).reshape(seq_rows, width_local)
    attn_part = jnp.dot(head_out, output_weight, preferred_element_type=jnp.float32)
    attn_sum = lax.psum(attn_part.astype(jnp.bfloat16), "tp").astype(jnp.float32)
    middle = residual + attn_sum
    ffn_in = rms_scale(middle, ffn_gain).astype(jnp.bfloat16)
    slice_width = dense_gate.shape[0]
    hidden_width = dense_gate.shape[1]
    own_columns = lax.dynamic_slice_in_dim(ffn_in, tp_index * slice_width, slice_width, 1)
    gate_up = jnp.concatenate((dense_gate, dense_up), axis=1)
    dense_part = jnp.dot(
        lax.all_gather(own_columns, "ep", axis=0, tiled=True),
        gate_up,
        preferred_element_type=jnp.float32,
    )
    dense_sum = lax.psum(dense_part.astype(jnp.bfloat16), "tp").astype(jnp.float32)
    dense_hidden = (jax.nn.silu(dense_sum[:, :hidden_width]) * dense_sum[:, hidden_width:]).astype(
        jnp.bfloat16
    )
    dense_out = lax.psum_scatter(
        jnp.dot(dense_hidden, dense_down, preferred_element_type=jnp.float32).astype(jnp.bfloat16),
        "ep",
        scatter_dimension=0,
        tiled=True,
    ).astype(jnp.float32)
    expert_count = lax.axis_size("ep")
    top_count = expert_ids.shape[1]
    capacity = max(2, 2 * seq_rows * top_count // expert_count)
    pair_ids = expert_ids.reshape(-1)
    onehot = (pair_ids[:, None] == jnp.arange(expert_count, dtype=jnp.int32)[None, :]).astype(
        jnp.int32
    )
    ranks = jnp.sum(onehot * (jnp.cumsum(onehot, axis=0) - 1), axis=1)
    places = pair_ids * capacity + ranks
    dispatch = (
        jnp.arange(expert_count * capacity, dtype=jnp.int32)[:, None] == places[None, :]
    ).astype(jnp.bfloat16)
    repeated = jnp.repeat(ffn_in, top_count, axis=0)
    outgoing = jnp.dot(dispatch, repeated, preferred_element_type=jnp.float32).astype(jnp.bfloat16)
    outgoing = outgoing.reshape(expert_count, capacity, ffn_in.shape[1])
    arrived = lax.all_to_all(outgoing, "ep", split_axis=0, concat_axis=0, tiled=True)
    gate_vals = jnp.einsum(
        "snd,df->snf", arrived, expert_gate[0], preferred_element_type=jnp.float32
    )
    up_vals = jnp.einsum("snd,df->snf", arrived, expert_up[0], preferred_element_type=jnp.float32)
    expert_hidden = (jax.nn.silu(gate_vals) * up_vals).astype(jnp.bfloat16)
    partial_value = jnp.einsum(
        "snf,fd->snd", expert_hidden, expert_down[0], preferred_element_type=jnp.float32
    )
    summed_cols = lax.psum_scatter(
        partial_value.astype(jnp.bfloat16), "tp", scatter_dimension=2, tiled=True
    )
    returned = lax.all_to_all(summed_cols, "ep", split_axis=0, concat_axis=0, tiled=True)
    flat_back = returned.reshape(expert_count * capacity, slice_width)
    picked = (
        jnp.take(flat_back, places, axis=0)
        .astype(jnp.float32)
        .reshape(seq_rows, top_count, slice_width)
    )
    logit_exp = jnp.exp(expert_logit)
    route_weight = group_prob[:, None] * logit_exp / jnp.sum(logit_exp, axis=1, keepdims=True)
    expert_mix = jnp.sum(route_weight[..., None] * picked, axis=1)
    own_middle = lax.dynamic_slice_in_dim(middle, tp_index * slice_width, slice_width, 1)
    mixed_out = (own_middle + jax.nn.sigmoid(dense_mix) * dense_out + expert_mix).astype(
        jnp.bfloat16
    )
    return (mixed_out, new_state)


def solution(mesh):
    return jax.shard_map(
        per_device,
        mesh=mesh,
        in_specs=(
            P("ep", None),
            P("ep", "tp", None, None),
            P(),
            P("ep", "tp"),
            P("ep", "tp"),
            P("ep", "tp"),
            P(),
            P(),
            P("tp"),
            P(),
            P("tp", None),
            P(),
            P("ep", None),
            P("ep"),
            P("ep", None),
            P("ep", None, "tp"),
            P("ep", None, "tp"),
            P("ep", "tp", None),
            P("tp", "ep"),
            P("tp", "ep"),
            P("ep", "tp"),
            P("tp"),
        ),
        out_specs=(P("ep", "tp"), P("ep", "tp", None, None)),
        check_vma=False,
    )
```

profile of v0, /device:TPU:0, one launch (start us, length us, event | category | flops | bytes accessed | tf_op | source)
XLA Modules:
  0.0 333.8 jit_solution(11705922929324244987)
XLA Ops:
  7.2 1.2 fusion.28
  8.4 1.1 fusion.30
  9.6 15.0 %all_to_all.29 = bf16[24,8,512]{2,0,1:T(8,128)(2,1)S(1)} all-to-all(bf16[24,8,512]{2,0,1:T(8,128)(2,1)S(1)} %bitcast.59), channel_id=1, replica_groups=mesh['ep'=8,'tp'=4] {'ep'}, dimensions={1} | all-to-all | bytes 393216 | tf_op jit(solution)/shard_map/all_to_all | solution.py:49
  24.6 2.7 convolution_convert_fusion.3
  27.4 1.0 fusion.48
  28.5 1.0 fusion.27
  30.1 58.6 %reduce-scatter.4.cloned.1.call-done = bf16[24,1536]{1,0:T(8,128)(2,1)} async-done(((bf16[192,1536]{1,0:T(8,128)(2,1)}), bf16[24,1536]{1,0:T(8,128)(2,1)}) %reduce-scatter.4.cloned.1.call-update) | async-done | bytes 73744 | tf_op jit(solution)/shard_map/reduce_scatter | solution.py:51
  88.8 0.8 fusion.58
  89.8 8.1 %fusion.59 = f32[24,4,1,128]{3,2,1,0:T(1,128)S(1)} fusion(f32[24,4,128,1]{2,3,1,0:T(1,128)S(1)} %bitcast.60, f32[24,4,128,128]{3,2,1,0:T(8,128)} %param.23), kind=kOutput, calls=%fused_computation.93 | convolution fusion | flops 18874368 | bytes 6389760 | tf_op jit(solution)/shard_map/bhk,bhkv->bhv/dot_general | solution.py:73
  98.1 3.9 %multiply_add_fusion = f32[24,4,128,128]{3,2,1,0:T(8,128)} fusion(f32[24,4,128,128]{3,2,1,0:T(8,128)S(1)} %copy-done.1, f32[24,4,128]{2,1,0:T(4,128)S(1)} %subtract_multiply_fusion, f32[24,4,128]{2,1,0:T(4,128)S(1)} %broadcast_multiply_fusion, f32[24,4]{1,0:T(8,128)S(1)} %copy.67), kind=kLoop, calls=%fused_computation.1 | loop fusion | flops 4718592 | bytes 12681600 | tf_op jit(solution)/shard_map/add | solution.py:76
  102.2 7.5 %fusion.60 = f32[24,4,1,128]{3,2,1,0:T(1,128)S(1)} fusion(f32[24,4,128,1]{2,3,1,0:T(1,128)S(1)} %bitcast.63, f32[24,4,128,128]{3,2,1,0:T(8,128)} %multiply_add_fusion), kind=kOutput, calls=%fused_computation.94 | convolution fusion | flops 18874368 | bytes 6389760 | tf_op jit(solution)/shard_map/bhk,bhkv->bhv/dot_general | solution.py:78
  109.9 1.4 convolution_convert_fusion.2
  111.3 31.2 %all-reduce.3.cloned.1.call-done = bf16[24,4096]{1,0:T(8,128)(2,1)} async-done(((bf16[24,4096]{1,0:T(8,128)(2,1)}), bf16[24,4096]{1,0:T(8,128)(2,1)}) %all-reduce.3.cloned.1.call-update) | async-done | bytes 196624 | tf_op jit(solution)/shard_map/psum | solution.py:81
  142.5 1.8 convert_add_fusion
  144.3 1.0 multiply_convert_fusion
  145.9 0.3 convolution_convert_fusion.1
  146.2 1.2 reshape.153
  147.4 5.5 %all-to-all-start.1 = ((bf16[8,12,4096]{2,1,0:T(8,128)(2,1)}), bf16[8,12,4096]{2,1,0:T(8,128)(2,1)S(1)}, u32[]{:S(2)}, u32[]{:S(2)}) async-start(bf16[8,12,4096]{2,1,0:T(8,128)(2,1)} %reshape.153), calls=%async_computation.3 | async-start | bytes 2097152 | tf_op jit(solution)/shard_map/all_to_all | solution.py:118
  153.0 45.7 %all_gather.3 = bf16[192,1024]{1,0:T(8,128)(2,1)S(1)} all-gather(bf16[24,1024]{1,0:T(8,128)(2,1)S(1)} %constant_dynamic-slice_fusion), channel_id=1, replica_groups=mesh['ep'=8,'tp'=4] {'ep'}, dimensions={0}, use_global_device_ids=true | all-gather | bytes 442368 | tf_op jit(solution)/shard_map/all_gather | solution.py:89
  198.6 2.9 fusion.14
  201.6 2.0 fusion.7
  203.7 3.9 %convolution_convert_fusion = bf16[8,12,4096]{2,1,0:T(8,128)(2,1)} fusion(bf16[1,256,4096]{2,1,0:T(8,128)(2,1)S(1)} %copy-done, bf16[8,12,4096]{2,1,0:T(8,128)(2,1)S(1)} %all-to-all-done.1, bf16[1,4096,256]{2,1,0:T(8,128)(2,1)} %param.38, f32[8,12,256]{2,1,0:T(8,128)S(1)} %fusion.7), kind=kOutput, calls=%fused_computation.2 | convolution fusion | flops 403193856 | bytes 5865472 | tf_op jit(solution)/shard_map/snf,fd->snd/dot_general | solution.py:124
  207.9 25.3 %all-reduce.5.cloned.1.call-done = bf16[192,1024]{1,0:T(8,128)(2,1)} async-done(((bf16[192,1024]{1,0:T(8,128)(2,1)}), bf16[192,1024]{1,0:T(8,128)(2,1)}) %all-reduce.5.cloned.1.call-update) | async-done | bytes 393232 | tf_op jit(solution)/shard_map/psum | solution.py:93
  233.2 1.1 convert_element_type.71
  234.3 2.4 convolution_convert_fusion.4
  236.9 23.5 %reduce-scatter.8.cloned.1.call-done = bf16[8,12,1024]{2,1,0:T(8,128)(2,1)} async-done(((bf16[8,12,4096]{2,1,0:T(8,128)(2,1)}), bf16[8,12,1024]{2,1,0:T(8,128)(2,1)}) %reduce-scatter.8.cloned.1.call-update) | async-done | bytes 196624 | tf_op jit(solution)/shard_map/reduce_scatter | solution.py:127
  260.4 5.5 %all-to-all-start.2 = ((bf16[8,12,1024]{2,1,0:T(8,128)(2,1)}), bf16[8,12,1024]{2,1,0:T(8,128)(2,1)S(1)}, u32[]{:S(2)}, u32[]{:S(2)}) async-start(bf16[8,12,1024]{2,1,0:T(8,128)(2,1)} %reduce-scatter.8.cloned.1.call-done), calls=%async_computation.5 | async-start | bytes 524288 | tf_op jit(solution)/shard_map/all_to_all | solution.py:130
  266.1 9.1 %all-to-all-done.2 = bf16[8,12,1024]{2,1,0:T(8,128)(2,1)S(1)} async-done(((bf16[8,12,1024]{2,1,0:T(8,128)(2,1)}), bf16[8,12,1024]{2,1,0:T(8,128)(2,1)S(1)}, u32[]{:S(2)}, u32[]{:S(2)}) %all-to-all-start.2) | async-done | bytes 196640 | tf_op jit(solution)/shard_map/all_to_all | solution.py:130
  275.2 0.7 gather_fusion
  276.0 0.4 multiply_reduce_fusion.1
  276.4 49.3 %reduce-scatter.6.cloned.1.call-done = bf16[24,1024]{1,0:T(8,128)(2,1)} async-done(((bf16[192,1024]{1,0:T(8,128)(2,1)}), bf16[24,1024]{1,0:T(8,128)(2,1)}) %reduce-scatter.6.cloned.1.call-update) | async-done | bytes 49168 | tf_op jit(solution)/shard_map/reduce_scatter | solution.py:97
  325.7 1.6 add_convert_fusion
  (76 shorter events, 3.1 us)
Async XLA Ops:
  7.2 196.5 %copy-start = (bf16[1,256,4096]{2,1,0:T(8,128)(2,1)S(1)}, bf16[1,256,4096]{2,1,0:T(8,128)(2,1)}, u32[]{:S(2)}) copy-start(bf16[1,256,4096]{2,1,0:T(8,128)(2,1)} %param.39) | copy-start | bytes 6291460
  7.2 81.6 %reduce-scatter.4.cloned.1.call-start = ((), (), s32[]{:S(2)}) async-start(), calls=%async_computation.6 | async-start | bytes 663552 | tf_op jit(solution)/shard_map/reduce_scatter | solution.py:51
  9.5 17.8 %copy-start.10 = (f32[4]{0:T(128)S(1)}, f32[4]{0:T(128)}, u32[]{:S(2)}) copy-start(f32[4]{0:T(128)} %param.30) | copy-start | bytes 52
  9.5 20.1 %copy-start.5 = (s32[24,2]{0,1:T(2,128)S(1)}, s32[24,2]{0,1:T(2,128)}, u32[]{:S(2)}) copy-start(s32[24,2]{0,1:T(2,128)} %param.34) | copy-start | bytes 580
  27.3 115.2 %all-reduce.3.cloned.1.call-start = ((), (), s32[]{:S(2)}) async-start(), calls=%async_computation.7 | async-start | bytes 393216 | tf_op jit(solution)/shard_map/psum | solution.py:81
  89.8 8.2 %copy-start.1 = (f32[24,4,128,128]{3,2,1,0:T(8,128)S(1)}, f32[24,4,128,128]{3,2,1,0:T(8,128)}, u32[]{:S(2)}) copy-start(f32[24,4,128,128]{3,2,1,0:T(8,128)} %param.23) | copy-start | bytes 18874372
  102.2 7.6 %copy-start.8 = (f32[128]{0:T(128)S(1)}, f32[128]{0:T(128)}, u32[]{:S(2)}) copy-start(f32[128]{0:T(128)} %param.31) | copy-start | bytes 1540
  102.2 7.7 %copy-start.2 = (bf16[512,4096]{1,0:T(8,128)(2,1)S(1)}, bf16[512,4096]{1,0:T(8,128)(2,1)}, u32[]{:S(2)}) copy-start(bf16[512,4096]{1,0:T(8,128)(2,1)} %param.32) | copy-start | bytes 12582916
  109.7 32.8 %copy-start.3 = (bf16[24,4096]{1,0:T(8,128)(2,1)S(1)}, bf16[24,4096]{1,0:T(8,128)(2,1)}, u32[]{:S(2)}) copy-start(bf16[24,4096]{1,0:T(8,128)(2,1)} %param.22) | copy-start | bytes 589828
  109.7 34.7 %copy-start.4 = (f32[4096]{0:T(1024)S(1)}, f32[4096]{0:T(1024)}, u32[]{:S(2)}) copy-start(f32[4096]{0:T(1024)} %param.33) | copy-start | bytes 49156
  147.4 54.2 %all-to-all-start.1 = ((bf16[8,12,4096]{2,1,0:T(8,128)(2,1)}), bf16[8,12,4096]{2,1,0:T(8,128)(2,1)S(1)}, u32[]{:S(2)}, u32[]{:S(2)}) async-start(bf16[8,12,4096]{2,1,0:T(8,128)(2,1)} %reshape.153), calls=%async_computation.3 | async-start | bytes 2097152 | tf_op jit(solution)/shard_map/all_to_all | solution.py:118
  152.9 80.3 %all-reduce.5.cloned.1.call-start = ((), (), s32[]{:S(2)}) async-start(), calls=%async_computation.8 | async-start | bytes 786432 | tf_op jit(solution)/shard_map/psum | solution.py:93
  201.5 58.9 %reduce-scatter.8.cloned.1.call-start = ((), (), s32[]{:S(2)}) async-start(), calls=%async_computation.10 | async-start | bytes 1310720 | tf_op jit(solution)/shard_map/reduce_scatter | solution.py:127
  203.7 4.2 %copy-start.7 = (f32[24,2]{0,1:T(2,128)S(1)}, f32[24,2]{0,1:T(2,128)}, u32[]{:S(2)}) copy-start(f32[24,2]{0,1:T(2,128)} %param.36) | copy-start | bytes 580
  203.7 4.2 %copy-start.9 = (f32[24]{0:T(128)S(1)}, f32[24]{0:T(128)}, u32[]{:S(2)}) copy-start(f32[24]{0:T(128)} %param.35) | copy-start | bytes 292
  207.6 58.5 %copy-start.6 = (f32[1024]{0:T(1024)S(1)}, f32[1024]{0:T(1024)}, u32[]{:S(2)}) copy-start(f32[1024]{0:T(1024)} %param.43) | copy-start | bytes 12292
  207.6 118.1 %reduce-scatter.6.cloned.1.call-start = ((), (), s32[]{:S(2)}) async-start(), calls=%async_computation.9 | async-start | bytes 442368 | tf_op jit(solution)/shard_map/reduce_scatter | solution.py:97
  260.4 14.8 %all-to-all-start.2 = ((bf16[8,12,1024]{2,1,0:T(8,128)(2,1)}), bf16[8,12,1024]{2,1,0:T(8,128)(2,1)S(1)}, u32[]{:S(2)}, u32[]{:S(2)}) async-start(bf16[8,12,1024]{2,1,0:T(8,128)(2,1)} %reduce-scatter.8.cloned.1.call-done), calls=%async_computation.5 | async-start | bytes 524288 | tf_op jit(solution)/shard_map/all_to_all | solution.py:130
Sparse Core Ops, SparseCore 0:
  27.4 61.3 reduce-scatter.3
  111.4 31.0 all-reduce.2
  201.7 31.4 all-reduce.4
  235.6 24.7 reduce-scatter.7
  263.5 62.1 reduce-scatter.5
where the time goes:
time: 335 us; the launch traced here: 334 us
  waiting for transfers between devices  197 us (59%)
  blocking collectives  60.7 us (18%)
  matrix products  33.2 us (10%)
  between operations  14.1 us (4%)
  other arithmetic  13.2 us (4%)
  starting transfers between devices  11.2 us (3%)
  local copies, waits for them, and re-layouts  4.25 us (1%)
    reduce_scatter x1, waiting for transfers between devices, per_device(): lax.psum_scatter(jnp.dot(spread, joined, preferred_element_type=jnp.float...  58.6 us
    reduce_scatter x1, waiting for transfers between devices, per_device(): lax.psum_scatter(jnp.dot(dense_hidden, dense_down, preferred_element_type...  49.3 us
    all_gather x1, blocking collectives, per_device(): lax.all_gather(own_columns, 'ep', axis=0, tiled=True)  45.7 us
    psum x1, waiting for transfers between devices, per_device(): lax.psum(attn_part.astype(jnp.bfloat16), 'tp').astype(jnp.float32)  31.2 us
    psum x1, waiting for transfers between devices, per_device(): lax.psum(dense_part.astype(jnp.bfloat16), 'tp').astype(jnp.float32)  25.3 us
    reduce_scatter x1, waiting for transfers between devices, per_device(): lax.psum_scatter(partial_value.astype(jnp.bfloat16), 'tp', scatter_dimens...  23.5 us
    all_to_all x1, blocking collectives, per_device(): lax.all_to_all(normed, 'ep', split_axis=1, concat_axis=0, tiled=True)  15 us
    all_to_all x1, waiting for transfers between devices, per_device(): lax.all_to_all(summed_cols, 'ep', split_axis=0, concat_axis=0, tiled=True)  9.06 us
  transfers between devices with their start and end apart: 7, of which 6 were waited for; matrix products, arithmetic and copies ran while one was open for 5% of the time, Pallas kernels for 0%

commit v1 on v0

v1 whole, which is shorter than its diff:
```python
import functools

import jax
import jax.numpy as jnp
from jax import lax
from jax.experimental import pallas as pl
from jax.experimental.pallas import tpu as pltpu
from jax.sharding import PartitionSpec as P

EPS = 1e-06
BF = jnp.bfloat16
F32 = jnp.float32
MESH = pl.DeviceIdType.MESH


def dot(left, right):
    return jnp.dot(left, right, preferred_element_type=F32)


def silu(values):
    return values / (1.0 + jnp.exp(-values))


def kernel(dims, *refs):
    n_ep, n_tp, rows, width, heads, slots, topk, n_in, n_weights = dims
    inputs, refs = refs[:n_in], refs[n_in:]
    (tokens, attn_gain, decay_rate, head_gain, ffn_gain, ids, group_prob, logit, mix) = inputs[:9]
    hbm = inputs[9:]
    out, key_out, corr_out, decay_out = refs[:4]
    held = refs[4 : 4 + n_weights]
    refs = refs[4 + n_weights :]
    state, w_decay, w_beta, w_q, w_k, w_v, w_o, w_dg, w_du, w_eg, w_eu, w_ed, w_dd = held
    (
        n_send, n_recv, q_send, q_recv, c_send, c_recv, kq, recall, head_out,
        a_send, a_recv, s_recv, middle_ref, x_all, g_all, d_send, d_recv, h_all,
        e_send, e_recv, f_send, f_recv, load_sem, ep_send, ep_recv, tp_send, tp_recv,
    ) = refs
    me = lax.axis_index("ep")
    my = lax.axis_index("tp")
    chunk = width // n_tp
    depth = width // n_ep
    batch = n_ep * rows
    local = heads * 128

    loads = [
        pltpu.make_async_copy(src, dst, load_sem.at[i])
        for i, (src, dst) in enumerate(zip(hbm, held))
    ]
    state_i, decay_i, beta_i, q_i, k_i, v_i, o_i, dg_i, du_i, eg_i, eu_i, ed_i, dd_i = range(13)
    order = (decay_i, beta_i, q_i, k_i, v_i, state_i, o_i, dg_i, du_i, eg_i, eu_i, ed_i, dd_i)

    ep_peers = [lax.rem(me + d, n_ep) for d in range(1, n_ep)]
    tp_peers = [lax.rem(my + d, n_tp) for d in range(1, n_tp)]
    barrier = pltpu.get_barrier_semaphore()
    for p in ep_peers:
        pl.semaphore_signal(barrier, inc=1, device_id=(p, my), device_id_type=MESH)
    for p in tp_peers:
        pl.semaphore_signal(barrier, inc=1, device_id=(me, p), device_id_type=MESH)
    for i in order:
        loads[i].start()

    def ep_copy(phase, src, dst, peer, source):
        return pltpu.make_async_remote_copy(
            src_ref=src, dst_ref=dst,
            send_sem=ep_send.at[phase, peer], recv_sem=ep_recv.at[phase, source],
            device_id=(peer, my), device_id_type=MESH,
        )

    def tp_copy(phase, src, dst, peer, source):
        return pltpu.make_async_remote_copy(
            src_ref=src, dst_ref=dst,
            send_sem=tp_send.at[phase, peer], recv_sem=tp_recv.at[phase, source],
            device_id=(me, peer), device_id_type=MESH,
        )

    def exchange(copy, phase, peers, mine, src_of, dst):
        for p in peers:
            copy(phase, src_of(p), dst.at[mine], p, mine).start()

        def arrived():
            for p in peers:
                done = copy(phase, src_of(p), dst.at[p], p, p)
                done.wait_recv()
                done.wait_send()

        return arrived

    x = tokens[...].astype(F32)
    mean_sq = jnp.mean(x * x, axis=-1, keepdims=True)
    normed = (x * lax.rsqrt(mean_sq + EPS) * attn_gain[...]).astype(BF)
    for p in range(n_ep):
        n_send[p] = normed[:, p * depth : (p + 1) * depth]
    pl.semaphore_wait(barrier, n_ep + n_tp - 2)
    wait_n = exchange(ep_copy, 0, ep_peers, me, lambda p: n_send.at[p], n_recv)
    n_recv[me] = n_send[me]

    logit_exp = jnp.exp(logit[...])
    route = group_prob[...] * logit_exp / jnp.sum(logit_exp, axis=1, keepdims=True)
    names = ids[...]
    for p in range(n_ep):
        coef = jnp.sum(jnp.where(names == p, route, 0.0), axis=1, keepdims=True)
        c_send[p] = jnp.broadcast_to(coef, (rows, 128))
    loads[decay_i].wait()
    loads[beta_i].wait()
    decay_pre = dot(normed, w_decay[...])
    beta_pre = dot(normed, w_beta[...])
    lane = lax.broadcasted_iota(jnp.int32, decay_pre.shape, 1)
    decays, betas = [], []
    for h in range(heads):
        mine = lane == my * heads + h
        d = jnp.sum(jnp.where(mine, decay_pre, 0.0), axis=1, keepdims=True)
        b = jnp.sum(jnp.where(mine, beta_pre, 0.0), axis=1, keepdims=True)
        soft = jnp.maximum(d, 0.0) + jnp.log1p(jnp.exp(-jnp.abs(d)))
        decays.append(jnp.exp(-decay_rate[:, h : h + 1] * soft))
        betas.append(1.0 / (1.0 + jnp.exp(-b)))
    for i in (q_i, k_i, v_i):
        loads[i].wait()

    wait_n()
    spread = n_recv[...].astype(F32).reshape(batch, depth).astype(BF)
    for j, w in enumerate((w_q, w_k, w_v)):
        part = dot(spread, w[...]).reshape(n_ep, rows, local)
        q_send[:, :, j * local : (j + 1) * local] = part.astype(BF)
    wait_q = exchange(ep_copy, 1, ep_peers, me, lambda p: q_send.at[p], q_recv)
    q_recv[me] = q_send[me]
    loads[state_i].wait()
    wait_q()
    wait_c = exchange(ep_copy, 2, ep_peers, me, lambda p: c_send.at[p], c_recv)
    c_recv[me] = c_send[me]

    summed = q_recv[0].astype(F32)
    for p in range(1, n_ep):
        summed = summed + q_recv[p].astype(F32)
    summed = summed.astype(BF).astype(F32)

    def head_of(which, h):
        return summed[:, which * local + h * 128 : which * local + (h + 1) * 128]

    def unit(values):
        return values * lax.rsqrt(jnp.sum(values * values, axis=-1, keepdims=True) + EPS)

    units = []
    for h in range(heads):
        q_unit = unit(head_of(0, h)) * 128 ** (-0.5)
        k_unit = unit(head_of(1, h))
        units.append((q_unit, k_unit))
        kq[:, h, :] = k_unit
        kq[:, heads + h, :] = q_unit

    def one_row(b, _):
        columns = kq[b].T
        for h in range(heads):
            block = state[b, h]
            recall[h, pl.ds(b, 1), :] = jnp.sum(columns[:, h : h + 1] * block, axis=0, keepdims=True)
            recall[heads + h, pl.ds(b, 1), :] = jnp.sum(
                columns[:, heads + h : heads + h + 1] * block, axis=0, keepdims=True
            )
        return 0

    lax.fori_loop(0, rows, one_row, 0)
    for h in range(heads):
        q_unit, k_unit = units[h]
        decay, beta = decays[h], betas[h]
        corr = beta * (head_of(2, h) - decay * recall[h])
        read = decay * recall[heads + h] + jnp.sum(q_unit * k_unit, axis=-1, keepdims=True) * corr
        read = read * lax.rsqrt(jnp.mean(read * read, axis=-1, keepdims=True) + EPS) * head_gain[...]
        head_out[:, h * 128 : (h + 1) * 128] = read.astype(BF)
        key_out[:, h, :] = k_unit
        corr_out[:, h, :] = corr
        decay_out[:, h, :] = jnp.broadcast_to(decay, (rows, 128))

    loads[o_i].wait()
    ho = head_out[...]
    for c in range(n_tp):
        a_send[c] = dot(ho, w_o[:, c * chunk : (c + 1) * chunk]).astype(BF)
    wait_a = exchange(tp_copy, 0, tp_peers, my, lambda p: a_send.at[p], a_recv)
    a_recv[my] = a_send[my]
    own = pl.ds(pl.multiple_of(my * chunk, 128), chunk)
    middle = tokens[:, own].astype(F32)
    wait_a()
    for p in range(n_tp):
        middle = middle + a_recv[p].astype(F32)
    middle_ref[...] = middle
    s_recv[my] = jnp.broadcast_to(jnp.sum(middle * middle, axis=-1, keepdims=True), (rows, 128))
    wait_s = exchange(tp_copy, 1, tp_peers, my, lambda p: s_recv.at[my], s_recv)
    wait_c()
    coef = c_recv[...].reshape(batch, 128)[:, :1]
    named = coef > 0.0
    tri = (
        lax.broadcasted_iota(jnp.int32, (batch, batch), 0)
        >= lax.broadcasted_iota(jnp.int32, (batch, batch), 1)
    ).astype(F32).astype(BF)
    flags = jnp.broadcast_to(jnp.where(named, 1.0, 0.0), (batch, 128)).astype(BF)
    rank = dot(tri, flags)[:, :1] - 1.0
    slot = lax.broadcasted_iota(jnp.int32, (batch, slots), 1).astype(F32)
    place = jnp.where((rank == slot) & named, 1.0, 0.0).astype(BF)
    wait_s()
    total = s_recv[0]
    for p in range(1, n_tp):
        total = total + s_recv[p]
    scale = lax.rsqrt(total[:, :1] / width + EPS)
    x_all[me] = (middle * scale * ffn_gain[:, own]).astype(BF)
    wait_x = exchange(ep_copy, 3, ep_peers, me, lambda p: x_all.at[me], x_all)
    for i in (dg_i, du_i, eg_i, eu_i, ed_i, dd_i):
        loads[i].wait()
    wait_x()

    xs = x_all[...].astype(F32).reshape(batch, chunk).astype(BF)
    g_all[my] = lax.dot_general(
        place, xs, (((0,), (0,)), ((), ())), preferred_element_type=F32
    ).astype(BF)
    wait_g = exchange(tp_copy, 2, tp_peers, my, lambda p: g_all.at[my], g_all)
    hidden = w_dg.shape[1]
    part_rows = batch // n_tp
    for j, w in enumerate((w_dg, w_du)):
        part = dot(xs, w[...]).reshape(n_tp, part_rows, hidden)
        d_send[:, :, j * hidden : (j + 1) * hidden] = part.astype(BF)
    wait_d = exchange(tp_copy, 3, tp_peers, my, lambda p: d_send.at[p], d_recv)
    d_recv[my] = d_send[my]

    wait_g()
    gate = jnp.zeros((slots, w_eg.shape[2]), F32)
    up = jnp.zeros((slots, w_eg.shape[2]), F32)
    for c in range(n_tp):
        gate = gate + dot(g_all[c], w_eg[0, c * chunk : (c + 1) * chunk, :])
        up = up + dot(g_all[c], w_eu[0, c * chunk : (c + 1) * chunk, :])
    expert_hidden = (silu(gate) * up).astype(BF)
    for c in range(n_tp):
        e_send[c] = dot(expert_hidden, w_ed[0, :, c * chunk : (c + 1) * chunk]).astype(BF)
    wait_e = exchange(tp_copy, 4, tp_peers, my, lambda p: e_send.at[p], e_recv)
    e_recv[my] = e_send[my]

    wait_d()
    pre = d_recv[0].astype(F32)
    for p in range(1, n_tp):
        pre = pre + d_recv[p].astype(F32)
    h_all[my] = (silu(pre[:, :hidden]) * pre[:, hidden:]).astype(BF)
    wait_h = exchange(tp_copy, 5, tp_peers, my, lambda p: h_all.at[my], h_all)
    wait_h()
    dense_hidden = h_all[...].astype(F32).reshape(batch, hidden).astype(BF)
    dense = dot(dense_hidden, w_dd[...]) * (1.0 / (1.0 + jnp.exp(-mix[...])))
    wait_e()
    result = e_recv[0].astype(F32)
    for p in range(1, n_tp):
        result = result + e_recv[p].astype(F32)
    combined = dense + coef * dot(place, result.astype(BF))
    f_send[...] = combined.reshape(n_ep, rows, chunk).astype(BF)
    wait_f = exchange(ep_copy, 4, ep_peers, me, lambda p: f_send.at[p], f_recv)
    final = middle_ref[...] + f_send[me].astype(F32)
    f_recv[me] = jnp.zeros((rows, chunk), BF)
    wait_f()
    for p in range(n_ep):
        final = final + f_recv[p].astype(F32)
    out[...] = final.astype(BF)


def per_device(
    tokens, delta_state, attn_gain, query_weight, key_weight, value_weight, decay_weight,
    beta_weight, decay_rate, head_gain, output_weight, ffn_gain, expert_ids, group_prob,
    expert_logit, expert_gate, expert_up, expert_down, dense_gate, dense_up, dense_down, dense_mix,
):
    n_ep = lax.axis_size("ep")
    n_tp = lax.axis_size("tp")
    rows, width = tokens.shape
    heads = delta_state.shape[1]
    local = heads * 128
    topk = expert_ids.shape[1]
    slots = max(2, 2 * rows * topk // n_ep) * n_ep
    chunk = width // n_tp
    depth = width // n_ep
    batch = n_ep * rows
    hidden = dense_gate.shape[1]
    small = (
        tokens, attn_gain[None, :], decay_rate[None, :], head_gain[None, :], ffn_gain[None, :],
        expert_ids, group_prob[:, None], expert_logit, dense_mix[None, :],
    )
    weights = (
        delta_state, decay_weight, beta_weight, query_weight, key_weight, value_weight,
        output_weight, dense_gate, dense_up, expert_gate, expert_up, expert_down, dense_down,
    )
    dims = (n_ep, n_tp, rows, width, heads, slots, topk, len(small) + len(weights), len(weights))
    vmem = pl.BlockSpec(memory_space=pltpu.VMEM)
    kq_rows = -(-2 * heads // 8) * 8
    scratch = [pltpu.VMEM(w.shape, w.dtype) for w in weights]
    scratch += [
        pltpu.VMEM(shape, dtype)
        for shape, dtype in (
            ((n_ep, rows, depth), BF), ((n_ep, rows, depth), BF),
            ((n_ep, rows, 3 * local), BF), ((n_ep, rows, 3 * local), BF),
            ((n_ep, rows, 128), F32), ((n_ep, rows, 128), F32),
            ((rows, kq_rows, 128), F32), ((2 * heads, rows, 128), F32), ((rows, local), BF),
            ((n_tp, rows, chunk), BF), ((n_tp, rows, chunk), BF), ((n_tp, rows, 128), F32),
            ((rows, chunk), F32), ((n_ep, rows, chunk), BF), ((n_tp, slots, chunk), BF),
            ((n_tp, batch // n_tp, 2 * hidden), BF), ((n_tp, batch // n_tp, 2 * hidden), BF),
            ((n_tp, batch // n_tp, hidden), BF),
            ((n_tp, slots, chunk), BF), ((n_tp, slots, chunk), BF),
            ((n_ep, rows, chunk), BF), ((n_ep, rows, chunk), BF),
        )
    ]
    scratch += [
        pltpu.SemaphoreType.DMA((len(weights),)),
        pltpu.SemaphoreType.DMA((5, n_ep)), pltpu.SemaphoreType.DMA((5, n_ep)),
        pltpu.SemaphoreType.DMA((6, n_tp)), pltpu.SemaphoreType.DMA((6, n_tp)),
    ]
    per_head = jax.ShapeDtypeStruct((rows, heads, 128), F32)
    mixed_out, key, corr, decay = pl.pallas_call(
        functools.partial(kernel, dims),
        out_shape=(jax.ShapeDtypeStruct((rows, chunk), BF), per_head, per_head, per_head),
        in_specs=[vmem] * len(small) + [pl.BlockSpec(memory_space=pl.ANY)] * len(weights),
        out_specs=(vmem,) * 4,
        scratch_shapes=scratch,
        compiler_params=pltpu.CompilerParams(
            collective_id=0, has_side_effects=True, vmem_limit_bytes=62 * 1024 * 1024
        ),
    )(*small, *weights)
    new_state = decay[:, :, None, :] * delta_state + key[..., :, None] * corr[..., None, :]
    return mixed_out, new_state


def solution(mesh):
    return jax.shard_map(
        per_device,
        mesh=mesh,
        in_specs=(
            P("ep", None), P("ep", "tp", None, None), P(), P("ep", "tp"), P("ep", "tp"),
            P("ep", "tp"), P(), P(), P("tp"), P(), P("tp", None), P(), P("ep", None), P("ep"),
            P("ep", None), P("ep", None, "tp"), P("ep", None, "tp"), P("ep", "tp", None),
            P("tp", "ep"), P("tp", "ep"), P("ep", "tp"), P("tp"),
        ),
        out_specs=(P("ep", "tp"), P("ep", "tp", None, None)),
        check_vma=False,
    )
```

time: 335 us -> 106 us (0.32)
  waiting for transfers between devices: 197 us -> 0 us
  Pallas kernels: 0 us -> 88.7 us
  blocking collectives: 60.7 us -> 0 us
  matrix products: 33.2 us -> 0 us
  between operations: 14.1 us -> 0.65 us
  starting transfers between devices: 11.2 us -> 0 us
  other arithmetic: 13.2 us -> 7.37 us
  local copies, waits for them, and re-layouts: 4.25 us -> 9.11 us
    reduce_scatter x3 -> x0, waiting for transfers between devices: 131 us -> none  [the longest x1 58.6 us: per_device(): lax.psum_scatter(jnp.dot(spread, joined, preferred_element_type=jnp.float...]
    pallas_call x0 -> x1, Pallas kernels: none -> 88.7 us  [per_device(): pl.pallas_call(functools.partial(kernel, dims), out_shape=(jax.ShapeDtype...]
    psum x2 -> x0, waiting for transfers between devices: 56.5 us -> none  [the longest x1 31.2 us: per_device(): lax.psum(attn_part.astype(jnp.bfloat16), 'tp').astype(jnp.float32)]
    all_gather x1 -> x0, blocking collectives: 45.7 us -> none  [per_device(): lax.all_gather(own_columns, 'ep', axis=0, tiled=True)]
    dot_general x11 -> x0, matrix products: 33.2 us -> none  [the longest x1 8.1 us: per_device(): jnp.einsum('bhk,bhkv->bhv', key_unit, delta_state, precision=lax.Precisio...]
    all_to_all x1 -> x0, blocking collectives: 15 us -> none  [per_device(): lax.all_to_all(normed, 'ep', split_axis=1, concat_axis=0, tiled=True)]
    all_to_all x2 -> x0, starting transfers between devices: 11 us -> none  [the longest x1 5.51 us: per_device(): lax.all_to_all(outgoing, 'ep', split_axis=0, concat_axis=0, tiled=True)]
    all_to_all x2 -> x0, waiting for transfers between devices: 9.06 us -> none  [the longest x1 9.06 us: per_device(): lax.all_to_all(summed_cols, 'ep', split_axis=0, concat_axis=0, tiled=True)]
  transfers between devices with their start and end apart: 7 -> 0, of which waited for: 6 -> 0; matrix products, arithmetic and copies ran while one was open for 5% -> 0% of each run, Pallas kernels for 0% -> 0%
where the time goes in v1:
time: 106 us
  Pallas kernels  88.7 us (84%)
  local copies, waits for them, and re-layouts  9.11 us (9%)
  other arithmetic  7.37 us (7%)
    pallas_call x1, Pallas kernels, per_device(): pl.pallas_call(functools.partial(kernel, dims), out_shape=(jax.ShapeDtype...  88.7 us
    unnamed x7, local copies, waits for them, and re-layouts  7.78 us
    add x1, other arithmetic, per_device(): decay[:, :, None, :] * delta_state + key[..., :, None] * corr[..., None, :]  7.37 us

profile of v1, /device:TPU:0, one launch (start us, length us, event | category | flops | bytes accessed | tf_op | source)
XLA Modules:
  0.0 105.8 jit_solution(11293629090306351799)
XLA Ops:
  0.6 1.4 %copy.24.refs_5_ = s32[24,2]{1,0:T(8,128)} copy(s32[24,2]{0,1:T(2,128)} %param.34) | data formatting | bytes 384 | tf_op args[12]
  2.0 1.3 %copy.25.refs_6_ = f32[24,1]{1,0:T(8,128)} copy(f32[24,1]{0,1:T(1,128)} %bitcast.11) | data formatting | bytes 192 | tf_op jit(solution)/shard_map/broadcast_in_dim | solution.py:275
  3.3 1.4 %copy.26.refs_7_ = f32[24,2]{1,0:T(8,128)} copy(f32[24,2]{0,1:T(2,128)} %param.36) | data formatting | bytes 384 | tf_op args[14]
  4.7 2.2 %copy.27.refs_10_ = bf16[4096,16]{1,0:T(8,128)(2,1)} copy(bf16[4096,16]{0,1:T(8,128)(2,1)} %param.28) | data formatting | bytes 262144 | tf_op args[6]
  6.9 2.2 %copy.28.refs_11_ = bf16[4096,16]{1,0:T(8,128)(2,1)} copy(bf16[4096,16]{0,1:T(8,128)(2,1)} %param.29) | data formatting | bytes 262144 | tf_op args[7]
  9.1 88.7 %shard_map.221 = (bf16[24,1024]{1,0:T(8,128)(2,1)}, f32[24,4,128]{2,1,0:T(4,128)}, f32[24,4,128]{2,1,0:T(4,128)}, f32[24,4,128]{2,1,0:T(4,128)}) custom-call(bf16[24,4096]{1,0:T(8,128)(2,1)} %refs_0_.1, f32[1,4096]{1,0:T(1,128)} %bitcast.6, f32[1,4]{1,0:T(1,128)} %bitcast.9, f32[1,128]{1,0:T(1,128)} %bitcast.10, f32[1,4096]{1,0:T(1,128)} %bitcast.7, ...), custom_call_target="tpu_custom_call" | custom-call | tf_op jit(solution)/shard_map/pallas_call | solution.py:306
  97.8 0.0 copy-start
  97.8 7.4 %multiply_add_fusion = f32[24,4,128,128]{3,2,1,0:T(8,128)} fusion(f32[24,4,128,128]{3,2,1,0:T(8,128)} %refs_9_.1, f32[24,4,128]{2,1,0:T(4,128)} %get-tuple-element.9, f32[24,4,128]{2,1,0:T(4,128)} %get-tuple-element.8, f32[24,4,128]{2,1,0:T(4,128)} %get-tuple-element.7), kind=kLoop, calls=%fused_computation | loop fusion | flops 4718592 | bytes 12730368 | tf_op jit(solution)/shard_map/add | solution.py:316
  105.2 0.0 copy-done
  105.2 0.6 copy.30
Async XLA Ops:
  97.8 7.4 %copy-start = (bf16[24,1024]{1,0:T(8,128)(2,1)S(1)}, bf16[24,1024]{1,0:T(8,128)(2,1)}, u32[]{:S(2)}) copy-start(bf16[24,1024]{1,0:T(8,128)(2,1)} %get-tuple-element.12) | copy-start | bytes 147460

commit v2 on v1

--- a/solution.py
+++ b/solution.py
@@ -1,4 +1,5 @@
 import functools
+import math
 
 import jax
 import jax.numpy as jnp
@@ -17,12 +18,28 @@
     return jnp.dot(left, right, preferred_element_type=F32)
 
 
+def dot_t(left, right):
+    return lax.dot_general(left, right, (((1,), (1,)), ((), ())), preferred_element_type=F32)
+
+
 def silu(values):
     return values / (1.0 + jnp.exp(-values))
 
 
+class BlockOf:
+    def __init__(self, ref, block):
+        self.ref, self.block = ref, block
+
+    @property
+    def at(self):
+        return self
+
+    def __getitem__(self, index):
+        return self.ref.at[index, self.block]
+
+
 def kernel(dims, *refs):
-    n_ep, n_tp, rows, width, heads, slots, topk, n_in, n_weights = dims
+    n_ep, n_tp, rows, width, heads, members, cap, n_in, n_weights = dims
     inputs, refs = refs[:n_in], refs[n_in:]
     (tokens, attn_gain, decay_rate, head_gain, ffn_gain, ids, group_prob, logit, mix) = inputs[:9]
     hbm = inputs[9:]
@@ -33,7 +50,7 @@
     (
         n_send, n_recv, q_send, q_recv, c_send, c_recv, kq, recall, head_out,
         a_send, a_recv, s_recv, middle_ref, x_all, g_all, d_send, d_recv, h_all,
-        e_send, e_recv, f_send, f_recv, load_sem, ep_send, ep_recv, tp_send, tp_recv,
+        e_send, e_recv, f_send, f_recv, place_ref, dense_ref, load_sem, ep_send, ep_recv, tp_send, tp_recv,
     ) = refs
     me = lax.axis_index("ep")
     my = lax.axis_index("tp")
@@ -41,6 +58,17 @@
     depth = width // n_ep
     batch = n_ep * rows
     local = heads * 128
+    groups = n_ep // members
+    group_slots = members * cap
+    group_tokens = members * rows
+    slots = groups * group_slots
+    my_group = lax.div(me, members)
+    my_member = lax.rem(me, members)
+
+    def members_of(offset):
+        first = lax.rem(my_group + offset + groups, groups) * members
+        start = 1 if offset == 0 else 0
+        return [first + lax.rem(my_member + m, members) for m in range(start, members)]
 
     loads = [
         pltpu.make_async_copy(src, dst, load_sem.at[i])
@@ -49,7 +77,7 @@
     state_i, decay_i, beta_i, q_i, k_i, v_i, o_i, dg_i, du_i, eg_i, eu_i, ed_i, dd_i = range(13)
     order = (decay_i, beta_i, q_i, k_i, v_i, state_i, o_i, dg_i, du_i, eg_i, eu_i, ed_i, dd_i)
 
-    ep_peers = [lax.rem(me + d, n_ep) for d in range(1, n_ep)]
+    ep_peers = [p for offset in range(groups) for p in members_of(offset)]
     tp_peers = [lax.rem(my + d, n_tp) for d in range(1, n_tp)]
     barrier = pltpu.get_barrier_semaphore()
     for p in ep_peers:
@@ -95,15 +123,19 @@
     n_recv[me] = n_send[me]
 
     logit_exp = jnp.exp(logit[...])
-    route = group_prob[...] * logit_exp / jnp.sum(logit_exp, axis=1, keepdims=True)
+    route = group_prob[...] * logit_exp / jnp.sum(logit_exp, axis=0, keepdims=True)
     names = ids[...]
+    eye = lax.broadcasted_iota(jnp.int32, (rows, rows), 0) == lax.broadcasted_iota(
+        jnp.int32, (rows, rows), 1
+    )
     for p in range(n_ep):
-        coef = jnp.sum(jnp.where(names == p, route, 0.0), axis=1, keepdims=True)
+        flat = jnp.sum(jnp.where(names == p, route, 0.0), axis=0, keepdims=True)
+        coef = jnp.sum(jnp.where(eye, flat, 0.0), axis=1, keepdims=True)
         c_send[p] = jnp.broadcast_to(coef, (rows, 128))
     loads[decay_i].wait()
     loads[beta_i].wait()
-    decay_pre = dot(normed, w_decay[...])
-    beta_pre = dot(normed, w_beta[...])
+    decay_pre = dot_t(normed, w_decay[...])
+    beta_pre = dot_t(normed, w_beta[...])
     lane = lax.broadcasted_iota(jnp.int32, decay_pre.shape, 1)
     decays, betas = [], []
     for h in range(heads):
@@ -118,31 +150,36 @@
 
     wait_n()
     spread = n_recv[...].astype(F32).reshape(batch, depth).astype(BF)
-    for j, w in enumerate((w_q, w_k, w_v)):
+    wait_heads = []
+    for j, w in enumerate((w_k, w_q, w_v)):
         part = dot(spread, w[...]).reshape(n_ep, rows, local)
-        q_send[:, :, j * local : (j + 1) * local] = part.astype(BF)
-    wait_q = exchange(ep_copy, 1, ep_peers, me, lambda p: q_send.at[p], q_recv)
-    q_recv[me] = q_send[me]
+        q_send[j] = part.astype(BF)
+        wait_heads.append(
+            exchange(ep_copy, 1 + j, ep_peers, me, lambda p, j=j: q_send.at[j, p], q_recv.at[j])
+        )
+        q_recv[j, me] = q_send[j, me]
+
+    def summed(j):
+        wait_heads[j]()
+        total = q_recv[j, 0].astype(F32)
+        for p in range(1, n_ep):
+            total = total + q_recv[j, p].astype(F32)
+        return total.astype(BF).astype(F32)
+
+    k_rows = summed(0)
+    q_rows = summed(1)
     loads[state_i].wait()
-    wait_q()
-    wait_c = exchange(ep_copy, 2, ep_peers, me, lambda p: c_send.at[p], c_recv)
-    c_recv[me] = c_send[me]
-
-    summed = q_recv[0].astype(F32)
-    for p in range(1, n_ep):
-        summed = summed + q_recv[p].astype(F32)
-    summed = summed.astype(BF).astype(F32)
-
-    def head_of(which, h):
-        return summed[:, which * local + h * 128 : which * local + (h + 1) * 128]
+
+    def head_of(values, h):
+        return values[:, h * 128 : (h + 1) * 128]
 
     def unit(values):
         return values * lax.rsqrt(jnp.sum(values * values, axis=-1, keepdims=True) + EPS)
 
     units = []
     for h in range(heads):
-        q_unit = unit(head_of(0, h)) * 128 ** (-0.5)
-        k_unit = unit(head_of(1, h))
+        q_unit = unit(head_of(q_rows, h)) * 128 ** (-0.5)
+        k_unit = unit(head_of(k_rows, h))
         units.append((q_unit, k_unit))
         kq[:, h, :] = k_unit
         kq[:, heads + h, :] = q_unit
@@ -158,10 +195,13 @@
         return 0
 
     lax.fori_loop(0, rows, one_row, 0)
+    v_rows = summed(2)
+    wait_c = exchange(ep_copy, 4, ep_peers, me, lambda p: c_send.at[p], c_recv)
+    c_recv[me] = c_send[me]
     for h in range(heads):
         q_unit, k_unit = units[h]
         decay, beta = decays[h], betas[h]
-        corr = beta * (head_of(2, h) - decay * recall[h])
+        corr = beta * (head_of(v_rows, h) - decay * recall[h])
         read = decay * recall[heads + h] + jnp.sum(q_unit * k_unit, axis=-1, keepdims=True) * corr
         read = read * lax.rsqrt(jnp.mean(read * read, axis=-1, keepdims=True) + EPS) * head_gain[...]
         head_out[:, h * 128 : (h + 1) * 128] = read.astype(BF)
@@ -184,71 +224,109 @@
     s_recv[my] = jnp.broadcast_to(jnp.sum(middle * middle, axis=-1, keepdims=True), (rows, 128))
     wait_s = exchange(tp_copy, 1, tp_peers, my, lambda p: s_recv.at[my], s_recv)
     wait_c()
-    coef = c_recv[...].reshape(batch, 128)[:, :1]
-    named = coef > 0.0
     tri = (
-        lax.broadcasted_iota(jnp.int32, (batch, batch), 0)
-        >= lax.broadcasted_iota(jnp.int32, (batch, batch), 1)
+        lax.broadcasted_iota(jnp.int32, (group_tokens, group_tokens), 0)
+        >= lax.broadcasted_iota(jnp.int32, (group_tokens, group_tokens), 1)
     ).astype(F32).astype(BF)
-    flags = jnp.broadcast_to(jnp.where(named, 1.0, 0.0), (batch, 128)).astype(BF)
-    rank = dot(tri, flags)[:, :1] - 1.0
-    slot = lax.broadcasted_iota(jnp.int32, (batch, slots), 1).astype(F32)
-    place = jnp.where((rank == slot) & named, 1.0, 0.0).astype(BF)
+    slot = lax.broadcasted_iota(jnp.int32, (group_tokens, group_slots), 1).astype(F32)
+    for g in range(groups):
+        coef = c_recv[g * members : (g + 1) * members].reshape(group_tokens, 128)[:, :1]
+        named = coef > 0.0
+        flags = jnp.broadcast_to(jnp.where(named, 1.0, 0.0), (group_tokens, 128)).astype(BF)
+        rank = dot(tri, flags)[:, :1] - 1.0
+        place_ref[g] = jnp.where((rank == slot) & named, 1.0, 0.0).astype(BF)
     wait_s()
     total = s_recv[0]
     for p in range(1, n_tp):
         total = total + s_recv[p]
     scale = lax.rsqrt(total[:, :1] / width + EPS)
     x_all[me] = (middle * scale * ffn_gain[:, own]).astype(BF)
-    wait_x = exchange(ep_copy, 3, ep_peers, me, lambda p: x_all.at[me], x_all)
+    for p in ep_peers:
+        ep_copy(5, x_all.at[me], x_all.at[me], p, me).start()
+    wait_g = []
+    for offset in range(groups):
+        g = lax.rem(my_group - offset + groups, groups)
+        for p in members_of(-offset):
+            ep_copy(5, x_all.at[me], x_all.at[p], p, p).wait_recv()
+        block = x_all[pl.ds(g * members, members)].astype(F32)
+        g_all[my, g] = lax.dot_general(
+            place_ref[g], block.reshape(group_tokens, chunk).astype(BF),
+            (((0,), (0,)), ((), ())), preferred_element_type=F32,
+        ).astype(BF)
+        wait_g.append(
+            exchange(
+                tp_copy, 4 + offset, tp_peers, my, lambda p, g=g: g_all.at[my, g],
+                BlockOf(g_all, g),
+            )
+        )
+    for p in ep_peers:
+        ep_copy(5, x_all.at[me], x_all.at[me], p, me).wait_send()
     for i in (dg_i, du_i, eg_i, eu_i, ed_i, dd_i):
         loads[i].wait()
-    wait_x()
-
     xs = x_all[...].astype(F32).reshape(batch, chunk).astype(BF)
-    g_all[my] = lax.dot_general(
-        place, xs, (((0,), (0,)), ((), ())), preferred_element_type=F32
-    ).astype(BF)
-    wait_g = exchange(tp_copy, 2, tp_peers, my, lambda p: g_all.at[my], g_all)
     hidden = w_dg.shape[1]
     part_rows = batch // n_tp
     for j, w in enumerate((w_dg, w_du)):
         part = dot(xs, w[...]).reshape(n_tp, part_rows, hidden)
         d_send[:, :, j * hidden : (j + 1) * hidden] = part.astype(BF)
-    wait_d = exchange(tp_copy, 3, tp_peers, my, lambda p: d_send.at[p], d_recv)
+    wait_d = exchange(tp_copy, 2, tp_peers, my, lambda p: d_send.at[p], d_recv)
     d_recv[my] = d_send[my]
 
-    wait_g()
+    for wait in wait_g:
+        wait()
     gate = jnp.zeros((slots, w_eg.shape[2]), F32)
     up = jnp.zeros((slots, w_eg.shape[2]), F32)
     for c in range(n_tp):
-        gate = gate + dot(g_all[c], w_eg[0, c * chunk : (c + 1) * chunk, :])
-        up = up + dot(g_all[c], w_eu[0, c * chunk : (c + 1) * chunk, :])
+        routed = g_all[c].astype(F32).reshape(slots, chunk).astype(BF)
+        gate = gate + dot(routed, w_eg[0, c * chunk : (c + 1) * chunk, :])
+        up = up + dot(routed, w_eu[0, c * chunk : (c + 1) * chunk, :])
     expert_hidden = (silu(gate) * up).astype(BF)
     for c in range(n_tp):
-        e_send[c] = dot(expert_hidden, w_ed[0, :, c * chunk : (c + 1) * chunk]).astype(BF)
-    wait_e = exchange(tp_copy, 4, tp_peers, my, lambda p: e_send.at[p], e_recv)
+        part = dot(expert_hidden, w_ed[0, :, c * chunk : (c + 1) * chunk])
+        e_send[c] = part.reshape(groups, group_slots, chunk).astype(BF)
     e_recv[my] = e_send[my]
-
+    returns = list(range(1, groups)) + [0]
+    group_at = [lax.rem(my_group + offset, groups) for offset in range(groups)]
+
+    def send_e(offset):
+        g = group_at[offset]
+        return exchange(
+            tp_copy, 4 + groups + offset, tp_peers, my, lambda p: e_send.at[p, g],
+            BlockOf(e_recv, g),
+        )
+
+    wait_e = {returns[0]: send_e(returns[0])}
     wait_d()
     pre = d_recv[0].astype(F32)
     for p in range(1, n_tp):
         pre = pre + d_recv[p].astype(F32)
     h_all[my] = (silu(pre[:, :hidden]) * pre[:, hidden:]).astype(BF)
-    wait_h = exchange(tp_copy, 5, tp_peers, my, lambda p: h_all.at[my], h_all)
+    wait_h = exchange(tp_copy, 3, tp_peers, my, lambda p: h_all.at[my], h_all)
+    for offset in returns[1:]:
+        wait_e[offset] = send_e(offset)
     wait_h()
     dense_hidden = h_all[...].astype(F32).reshape(batch, hidden).astype(BF)
     dense = dot(dense_hidden, w_dd[...]) * (1.0 / (1.0 + jnp.exp(-mix[...])))
-    wait_e()
-    result = e_recv[0].astype(F32)
-    for p in range(1, n_tp):
-        result = result + e_recv[p].astype(F32)
-    combined = dense + coef * dot(place, result.astype(BF))
-    f_send[...] = combined.reshape(n_ep, rows, chunk).astype(BF)
-    wait_f = exchange(ep_copy, 4, ep_peers, me, lambda p: f_send.at[p], f_recv)
+    dense_ref[...] = dense.reshape(n_ep, rows, chunk)
+    for offset in returns:
+        g = group_at[offset]
+        here = pl.ds(g * members, members)
+        wait_e[offset]()
+        result = e_recv[0, g].astype(F32)
+        for p in range(1, n_tp):
+            result = result + e_recv[p, g].astype(F32)
+        coef = c_recv[here].reshape(group_tokens, 128)[:, :1]
+        mixed = coef * dot(place_ref[g], result.astype(BF))
+        combined = dense_ref[here] + mixed.reshape(members, rows, chunk)
+        f_send[here] = combined.astype(BF)
+        for p in members_of(offset):
+            ep_copy(6, f_send.at[p], f_recv.at[me], p, me).start()
     final = middle_ref[...] + f_send[me].astype(F32)
     f_recv[me] = jnp.zeros((rows, chunk), BF)
-    wait_f()
+    for p in ep_peers:
+        done = ep_copy(6, f_send.at[p], f_recv.at[p], p, p)
+        done.wait_recv()
+        done.wait_send()
     for p in range(n_ep):
         final = final + f_recv[p].astype(F32)
     out[...] = final.astype(BF)
@@ -265,20 +343,25 @@
     heads = delta_state.shape[1]
     local = heads * 128
     topk = expert_ids.shape[1]
-    slots = max(2, 2 * rows * topk // n_ep) * n_ep
+    cap = max(2, 2 * rows * topk // n_ep)
+    members = 8 // math.gcd(cap, 8)
+    if n_ep % members:
+        members = n_ep
+    groups = n_ep // members
+    group_slots = members * cap
     chunk = width // n_tp
     depth = width // n_ep
     batch = n_ep * rows
     hidden = dense_gate.shape[1]
     small = (
         tokens, attn_gain[None, :], decay_rate[None, :], head_gain[None, :], ffn_gain[None, :],
-        expert_ids, group_prob[:, None], expert_logit, dense_mix[None, :],
+        expert_ids.T, group_prob[None, :], expert_logit.T, dense_mix[None, :],
     )
     weights = (
-        delta_state, decay_weight, beta_weight, query_weight, key_weight, value_weight,
+        delta_state, decay_weight.T, beta_weight.T, query_weight, key_weight, value_weight,
         output_weight, dense_gate, dense_up, expert_gate, expert_up, expert_down, dense_down,
     )
-    dims = (n_ep, n_tp, rows, width, heads, slots, topk, len(small) + len(weights), len(weights))
+    dims = (n_ep, n_tp, rows, width, heads, members, cap, len(small) + len(weights), len(weights))
     vmem = pl.BlockSpec(memory_space=pltpu.VMEM)
     kq_rows = -(-2 * heads // 8) * 8
     scratch = [pltpu.VMEM(w.shape, w.dtype) for w in weights]
@@ -286,21 +369,22 @@
         pltpu.VMEM(shape, dtype)
         for shape, dtype in (
             ((n_ep, rows, depth), BF), ((n_ep, rows, depth), BF),
-            ((n_ep, rows, 3 * local), BF), ((n_ep, rows, 3 * local), BF),
+            ((3, n_ep, rows, local), BF), ((3, n_ep, rows, local), BF),
             ((n_ep, rows, 128), F32), ((n_ep, rows, 128), F32),
             ((rows, kq_rows, 128), F32), ((2 * heads, rows, 128), F32), ((rows, local), BF),
             ((n_tp, rows, chunk), BF), ((n_tp, rows, chunk), BF), ((n_tp, rows, 128), F32),
-            ((rows, chunk), F32), ((n_ep, rows, chunk), BF), ((n_tp, slots, chunk), BF),
+            ((rows, chunk), F32), ((n_ep, rows, chunk), BF), ((n_tp, groups, group_slots, chunk), BF),
             ((n_tp, batch // n_tp, 2 * hidden), BF), ((n_tp, batch // n_tp, 2 * hidden), BF),
             ((n_tp, batch // n_tp, hidden), BF),
-            ((n_tp, slots, chunk), BF), ((n_tp, slots, chunk), BF),
+            ((n_tp, groups, group_slots, chunk), BF), ((n_tp, groups, group_slots, chunk), BF),
             ((n_ep, rows, chunk), BF), ((n_ep, rows, chunk), BF),
+            ((groups, members * rows, group_slots), BF), ((n_ep, rows, chunk), F32),
         )
     ]
     scratch += [
         pltpu.SemaphoreType.DMA((len(weights),)),
-        pltpu.SemaphoreType.DMA((5, n_ep)), pltpu.SemaphoreType.DMA((5, n_ep)),
-        pltpu.SemaphoreType.DMA((6, n_tp)), pltpu.SemaphoreType.DMA((6, n_tp)),
+        pltpu.SemaphoreType.DMA((7, n_ep)), pltpu.SemaphoreType.DMA((7, n_ep)),
+        pltpu.SemaphoreType.DMA((4 + 2 * groups, n_tp)), pltpu.SemaphoreType.DMA((4 + 2 * groups, n_tp)),
     ]
     per_head = jax.ShapeDtypeStruct((rows, heads, 128), F32)
     mixed_out, key, corr, decay = pl.pallas_call(

time: 106 us -> 87.2 us (0.82)
  Pallas kernels: 88.7 us -> 78.3 us
  local copies, waits for them, and re-layouts: 9.11 us -> 0.62 us
    pallas_call x1, Pallas kernels: 88.7 us -> 78.3 us  [per_device(): pl.pallas_call(functools.partial(kernel, dims), out_shape=(jax.ShapeDtype...]
    unnamed x7 -> x3, local copies, waits for them, and re-layouts: 7.78 us -> 0.62 us
    broadcast_in_dim x1 -> x0, local copies, waits for them, and re-layouts: 1.33 us -> none  [per_device(): group_prob[:, None]]
where the time goes in v2:
time: 87.2 us; the launch traced here: 87 us
  Pallas kernels  78.3 us (90%)
  other arithmetic  7.37 us (8%)
    pallas_call x1, Pallas kernels, per_device(): pl.pallas_call(functools.partial(kernel, dims), out_shape=(jax.ShapeDtype...  78.3 us
    add x1, other arithmetic, per_device(): decay[:, :, None, :] * delta_state + key[..., :, None] * corr[..., None, :]  7.37 us

profile of v2, /device:TPU:0, one launch (start us, length us, event | category | flops | bytes accessed | tf_op | source)
XLA Modules:
  0.0 87.0 jit_solution(17993009548093498984)
XLA Ops:
  0.6 78.3 %shard_map.221 = (bf16[24,1024]{1,0:T(8,128)(2,1)}, f32[24,4,128]{2,1,0:T(4,128)}, f32[24,4,128]{2,1,0:T(4,128)}, f32[24,4,128]{2,1,0:T(4,128)}) custom-call(bf16[24,4096]{1,0:T(8,128)(2,1)} %refs_0_.1, f32[1,4096]{1,0:T(1,128)} %bitcast.12, f32[1,4]{1,0:T(1,128)} %bitcast.17, f32[1,128]{1,0:T(1,128)} %bitcast.18, f32[1,4096]{1,0:T(1,128)} %bitcast.13, ...), custom_call_target="tpu_custom_call" | custom-call | tf_op jit(solution)/shard_map/pallas_call | solution.py:390
  79.0 0.0 copy-start
  79.0 7.4 %multiply_add_fusion = f32[24,4,128,128]{3,2,1,0:T(8,128)} fusion(f32[24,4,128,128]{3,2,1,0:T(8,128)} %refs_9_.1, f32[24,4,128]{2,1,0:T(4,128)} %get-tuple-element.9, f32[24,4,128]{2,1,0:T(4,128)} %get-tuple-element.8, f32[24,4,128]{2,1,0:T(4,128)} %get-tuple-element.7), kind=kLoop, calls=%fused_computation | loop fusion | flops 4718592 | bytes 12730368 | tf_op jit(solution)/shard_map/add | solution.py:400
  86.4 0.0 copy-done
  86.4 0.6 copy.25
Async XLA Ops:
  79.0 7.4 %copy-start = (bf16[24,1024]{1,0:T(8,128)(2,1)S(1)}, bf16[24,1024]{1,0:T(8,128)(2,1)}, u32[]{:S(2)}) copy-start(bf16[24,1024]{1,0:T(8,128)(2,1)} %get-tuple-element.12) | copy-start | bytes 147460
